TPU v7x, 32 devices: a whole 2x2x4 slice. The times are simulated.
32 devices in a mesh: grp: 2 (over y), sp: 4 (over z), tp: 4 (over x, core).
Axes of the slice: x: 2, y: 2, z: 4, core: 2. Of those that a mesh axis runs over, the one named last changes fastest.
Arguments:
- stream: bfloat16 [2048, 2048], P(('grp', 'sp'), 'tp'), parts along dimension 0, may hold values from -1.5 to 1.5
- layer_norm_gain: float32 [2, 2048], replicated, may hold values from 0.1 to 1.9
- convolution_in_weight: bfloat16 [2, 2048, 1536], P(None, 'sp', 'tp'), may hold values from -0.125 to 0.125
- gating_in_weight: bfloat16 [2, 2048, 1536], P(None, 'sp', 'tp'), may hold values from -0.125 to 0.125
- output_weight: bfloat16 [2, 1536, 2048], P(None, 'tp', 'sp'), may hold values from -0.15625 to 0.15625
- convolution_kernel_taps: float32 [2, 4, 1536], P(None, None, 'tp'), may hold values from -12 to 12
- recurrent_gate_blocks: bfloat16 [2, 2, 2, 12, 128, 128], P(None, None, None, 'tp'), may hold values from -0.5 to 0.5
- channel_decay_logit: float32 [2, 2, 1536], P(None, None, 'tp')
- position_decay_boost: float32 [2, 2, 2048], P(None, None, ('grp', 'sp')), parts along dimension 2, may hold values from -1.4 to 0, as said below
Outputs:
- new_stream: bfloat16 [2048, 2048], P(('grp', 'sp'), 'tp'), parts along dimension 0
There are 2 independent parts, one for each index of `grp`. A program takes and returns all parts, laid end to end along the dimension named above; an argument that names none is the same for every part. Nothing has to cross between parts.
Inputs may be any that keep to these rules, and one draw needn't show every extreme that they name: `position_decay_boost`: zero at all but a few positions.
All inputs are finite; a program needn't handle non-finite values.
Results may differ from a plain program's by a relative error of at most 0.025.
Values may be sent and summed in bfloat16 or wider, within the bound.
A program may use at most 128 MiB of HBM per device.

v0:
```python
import jax
import jax.numpy as jnp
from jax import lax
from jax.sharding import PartitionSpec as P

EPS = 1e-06
RECURRENT_WIDTH = 8.0


def extended(cells, sides, width):
    for axis, dim in sides:
        count = lax.axis_size(axis)
        ends = count - 1
        head = lax.slice_in_dim(cells, 0, width, axis=dim)
        tail = lax.slice_in_dim(cells, cells.shape[dim] - width, cells.shape[dim], axis=dim)
        cells = jnp.concatenate(
            [
                lax.ppermute(tail, axis, [(i, (i + 1) % count) for i in range(ends)]),
                cells,
                lax.ppermute(head, axis, [((i + 1) % count, i) for i in range(ends)]),
            ],
            axis=dim,
        )
    return cells


def entering(ends, place, count):
    forward = jnp.zeros_like(ends[0, :1])
    backward = forward
    for step in range(count - 1):
        forward = jnp.where(step < place, ends[step, 0:1] * forward + ends[step, 1:2], forward)
        source = count - 1 - step
        backward = jnp.where(
            source > place, ends[source, 2:3] * backward + ends[source, 3:4], backward
        )
    return (forward, backward)


def rms_norm(values, gain_row):
    floats = values.astype(jnp.float32)
    inverse = lax.rsqrt(jnp.mean(floats * floats, axis=-1, keepdims=True) + EPS)
    return (floats * inverse * gain_row).astype(jnp.bfloat16)


def combine_pairs(earlier, latter):
    return (earlier[0] * latter[0], latter[0] * earlier[1] + latter[1])


def local(
    stream,
    layer_norm_gain,
    convolution_in_weight,
    gating_in_weight,
    output_weight,
    convolution_kernel_taps,
    recurrent_gate_blocks,
    channel_decay_logit,
    position_decay_boost,
):
    tok_rows = stream.shape[0]
    channels = convolution_in_weight.shape[2]
    gate_count = recurrent_gate_blocks.shape[3]
    block_width = recurrent_gate_blocks.shape[4]
    seq_devices = lax.axis_size("sp")
    my_index = lax.axis_index("sp")
    seq_length = tok_rows * seq_devices
    positions = my_index * tok_rows + lax.iota(jnp.int32, tok_rows)
    at_first = (positions == 0)[:, None]
    at_last = (positions == seq_length - 1)[:, None]
    for layer_index in range(convolution_in_weight.shape[0]):
        features = lax.all_gather(stream, "tp", axis=1, tiled=True)
        normed = rms_norm(features, layer_norm_gain[layer_index])
        acc_x = jnp.dot(
            normed,
            lax.all_gather(convolution_in_weight[layer_index], "sp", axis=0, tiled=True),
            preferred_element_type=jnp.float32,
        )
        acc_y = jnp.dot(
            normed,
            lax.all_gather(gating_in_weight[layer_index], "sp", axis=0, tiled=True),
            preferred_element_type=jnp.float32,
        )
        proj_x = acc_x.astype(jnp.bfloat16)
        proj_y = acc_y.astype(jnp.bfloat16)
        padded = extended(proj_x, (("sp", 0),), 2).astype(jnp.float32)
        taps_now = convolution_kernel_taps[layer_index]
        conv_mixed = (
            taps_now[0] * padded[1 : tok_rows + 1]
            + taps_now[1] * padded[2 : tok_rows + 2]
            + taps_now[2] * padded[3 : tok_rows + 3]
            + taps_now[3] * padded[4 : tok_rows + 4]
        )
        convolution_output = conv_mixed.astype(jnp.bfloat16)
        conv_float = convolution_output.astype(jnp.float32)
        grouped = convolution_output.reshape(tok_rows, gate_count, block_width)
        results = []
        for scan_direction in range(2):
            gate_matrix_pair = recurrent_gate_blocks[layer_index, scan_direction]
            recurrent_branch = jax.nn.sigmoid(
                jnp.einsum(
                    "tnc,ncd->tnd", grouped, gate_matrix_pair[0], preferred_element_type=jnp.float32
                ).reshape(tok_rows, channels)
            )
            input_gate = jax.nn.sigmoid(
                jnp.einsum(
                    "tnc,ncd->tnd", grouped, gate_matrix_pair[1], preferred_element_type=jnp.float32
                ).reshape(tok_rows, channels)
            )
            decay_logarithm = (
                -RECURRENT_WIDTH
                * jax.nn.softplus(-channel_decay_logit[layer_index, scan_direction])
                * recurrent_branch
                + position_decay_boost[layer_index, scan_direction][:, None]
            )
            is_start = at_first if scan_direction == 0 else at_last
            multiplier = jnp.where(is_start, 1.0, jnp.sqrt(-jnp.expm1(2.0 * decay_logarithm)))
            driven = multiplier * input_gate * conv_float
            results.append(
                lax.associative_scan(
                    combine_pairs,
                    (jnp.exp(decay_logarithm), driven),
                    reverse=scan_direction == 1,
                    axis=0,
                )
            )
        cum_fwd, local_fwd = results[0]
        cum_bwd, local_bwd = results[1]
        ends = jnp.concatenate([cum_fwd[-1:], local_fwd[-1:], cum_bwd[:1], local_bwd[:1]], axis=0)
        enter_fwd, enter_bwd = entering(lax.all_gather(ends, "sp"), my_index, seq_devices)
        state_sum = local_fwd + cum_fwd * enter_fwd + local_bwd + cum_bwd * enter_bwd
        gated = (state_sum * jax.nn.gelu(proj_y.astype(jnp.float32))).astype(jnp.bfloat16)
        partials = jnp.dot(
            gated,
            lax.all_gather(output_weight[layer_index], "sp", axis=1, tiled=True),
            preferred_element_type=jnp.float32,
        ).astype(jnp.bfloat16)
        branch_sum = lax.psum_scatter(
            partials.astype(jnp.float32).astype(jnp.bfloat16), "tp", scatter_dimension=1, tiled=True
        ).astype(jnp.float32)
        stream = (stream.astype(jnp.float32) + branch_sum).astype(jnp.bfloat16)
    return stream


def solution(mesh):
    return jax.shard_map(
        local,
        mesh=mesh,
        in_specs=(
            P(("grp", "sp"), "tp"),
            P(),
            P(None, "sp", "tp"),
            P(None, "sp", "tp"),
            P(None, "tp", "sp"),
            P(None, None, "tp"),
            P(None, None, None, "tp", None, None),
            P(None, None, "tp"),
            P(None, None, ("grp", "sp")),
        ),
        out_specs=P(("grp", "sp"), "tp"),
        check_vma=False,
    )
```

profile of v0, /device:TPU:0, one launch (start us, length us, event | category | flops | bytes accessed | tf_op | source)
XLA Modules:
  0.0 339.8 jit_solution(17607182247680082666)
XLA Ops:
  6.5 0.7 all-gather.19.cloned.1.call-update
  7.3 2.1 fusion.210
  9.5 1.0 fusion.211
  10.7 1.0 fusion.212
  12.4 0.6 slice_reduce_fusion.19
  14.2 0.6 fusion.176
  14.8 13.5 %all-gather.19.cloned.1.call-done = bf16[256,2048]{1,0:T(8,128)(2,1)} async-done(((bf16[256,512]{1,0:T(8,128)(2,1)}), bf16[256,2048]{1,0:T(8,128)(2,1)}) %all-gather.19.cloned.1.call-update) | async-done | bytes 1048592 | tf_op jit(solution)/shard_map/all_gather | solution.py:71
  28.3 1.5 fusion
  29.9 37.1 %all-gather.23.cloned.1.call-done = bf16[1,2048,384]{2,1,0:T(8,128)(2,1)} async-done(((bf16[1,512,384]{2,1,0:T(8,128)(2,1)}), bf16[1,2048,384]{2,1,0:T(8,128)(2,1)}) %all-gather.23.cloned.1.call-update) | async-done | bytes 1572880 | tf_op jit(solution)/shard_map/all_gather | solution.py:75
  67.0 2.5 fusion.40
  69.5 2.6 collective-permute-start
  72.1 1.3 collective-permute-start.1
  74.0 3.6 %collective-permute-done.1 = bf16[2,384]{1,0:T(2,128)(2,1)S(1)} collective-permute-done((bf16[2,384]{1,0:T(2,128)(2,1)S(1)}, bf16[2,384]{1,0:T(2,128)(2,1)S(1)}, u32[]{:S(2)}, u32[]{:S(2)}) %collective-permute-start.1) | collective-permute-done | bytes 1568 | tf_op jit(solution)/shard_map/ppermute | solution.py:20
  80.0 1.6 convert_multiply_fusion.7
  88.5 0.7 fusion.142
  89.2 0.7 add.983
  89.9 0.7 add.996
  90.6 0.6 add.1019
  92.4 0.9 pad.453
  93.7 0.7 add.1021
  94.5 1.0 pad.455
  95.5 0.7 pad_maximum_fusion.3
  96.3 1.0 pad.454
  97.3 0.8 copy-done.6
  98.1 0.8 add.1023
  98.9 4.0 %rev.16 = f32[256,384]{1,0:T(8,128)} reverse(f32[256,384]{1,0:T(8,128)} %add.1023), dimensions={0} | reverse | bytes 786432 | tf_op jit(solution)/shard_map/rev | solution.py:119
  102.8 0.8 add.998
  103.6 3.9 %rev.17 = f32[256,384]{1,0:T(8,128)} reverse(f32[256,384]{1,0:T(8,128)} %add.998), dimensions={0} | reverse | bytes 786432 | tf_op jit(solution)/shard_map/rev | solution.py:119
  107.5 0.7 slice_add_fusion.12
  108.3 13.6 %all-gather.8 = f32[4,4,384]{2,1,0:T(4,128)S(1)} all-gather(f32[1,4,384]{2,1,0:T(4,128)S(1)} %maximum_bitcast_fusion), channel_id=3, replica_groups=mesh['grp'=2,'sp'=4,'tp'=4] {'sp'}, dimensions={0}, use_global_device_ids=true | all-gather | bytes 30720 | tf_op jit(solution)/shard_map/all_gather | solution.py:129
  122.0 20.0 %all-gather.27.cloned.1.call-done = bf16[1,384,2048]{2,1,0:T(8,128)(2,1)} async-done(((bf16[1,384,512]{2,1,0:T(8,128)(2,1)}), bf16[1,384,2048]{2,1,0:T(8,128)(2,1)}) %all-gather.27.cloned.1.call-update) | async-done | bytes 1572880 | tf_op jit(solution)/shard_map/all_gather | solution.py:134
  142.0 4.7 %convolution_convert_fusion.1 = bf16[256,2048]{1,0:T(8,128)(2,1)} fusion(bf16[1,384,2048]{2,1,0:T(8,128)(2,1)} %all-gather.27.cloned.1.call-done, bf16[1,2048,384]{2,1,0:T(8,128)(2,1)} %all-gather.25.cloned.1.call-done, f32[256,384]{1,0:T(8,128)} %rev.17, f32[256,384]{1,0:T(8,128)} %rev.16, f32[256,384]{1,0:T(8,128)S(1)} %pad.422, f32[256,384]{1,0:T(8,128)S(1)} %pad.423, ...), kind=kOutput, calls=%fused_computation.5 | convolution fusion | flops 809795584 | bytes 7614464 | tf_op jit(solution)/shard_map/dot_general | solution.py:132
  146.7 23.7 %reduce-scatter.3.cloned.1.call-done = bf16[256,512]{1,0:T(8,128)(2,1)} async-done(((bf16[256,2048]{1,0:T(8,128)(2,1)}), bf16[256,512]{1,0:T(8,128)(2,1)}) %reduce-scatter.3.cloned.1.call-update) | async-done | bytes 262160 | tf_op jit(solution)/shard_map/reduce_scatter | solution.py:137
  170.5 1.7 add_convert_fusion.1
  172.2 0.7 all-gather.29.cloned.1.call-update
  173.7 0.7 all-gather.33.cloned.1.call-update
  174.5 14.5 %all-gather.21.cloned.1.call-done = bf16[256,2048]{1,0:T(8,128)(2,1)} async-done(((bf16[256,512]{1,0:T(8,128)(2,1)}), bf16[256,2048]{1,0:T(8,128)(2,1)}) %all-gather.21.cloned.1.call-update) | async-done | bytes 1048592 | tf_op jit(solution)/shard_map/all_gather | solution.py:71
  189.0 1.5 fusion.3
  190.6 37.1 %all-gather.29.cloned.1.call-done = bf16[1,2048,384]{2,1,0:T(8,128)(2,1)} async-done(((bf16[1,512,384]{2,1,0:T(8,128)(2,1)}), bf16[1,2048,384]{2,1,0:T(8,128)(2,1)}) %all-gather.29.cloned.1.call-update) | async-done | bytes 1572880 | tf_op jit(solution)/shard_map/all_gather | solution.py:75
  227.7 2.5 fusion.49
  230.2 2.6 collective-permute-start.2
  232.8 1.3 collective-permute-start.3
  234.8 3.6 %collective-permute-done.3 = bf16[2,384]{1,0:T(2,128)(2,1)S(1)} collective-permute-done((bf16[2,384]{1,0:T(2,128)(2,1)S(1)}, bf16[2,384]{1,0:T(2,128)(2,1)S(1)}, u32[]{:S(2)}, u32[]{:S(2)}) %collective-permute-start.3) | collective-permute-done | bytes 1568 | tf_op jit(solution)/shard_map/ppermute | solution.py:20
  240.7 1.6 convert_multiply_fusion.5
  248.6 0.7 fusion.140
  249.3 0.7 add.1077
  250.0 0.6 add.1090
  250.7 0.6 add.1113
  252.5 0.9 pad.517
  253.8 0.7 add.1115
  254.6 1.0 pad.519
  255.6 0.7 pad_maximum_fusion.7
  256.3 1.0 pad.518
  257.4 0.8 copy-done.5
  258.1 0.8 add.1117
  258.9 4.0 %rev.18 = f32[256,384]{1,0:T(8,128)} reverse(f32[256,384]{1,0:T(8,128)} %add.1117), dimensions={0} | reverse | bytes 786432 | tf_op jit(solution)/shard_map/rev | solution.py:119
  262.9 0.8 add.1092
  263.7 3.8 %rev.19 = f32[256,384]{1,0:T(8,128)} reverse(f32[256,384]{1,0:T(8,128)} %add.1092), dimensions={0} | reverse | bytes 786432 | tf_op jit(solution)/shard_map/rev | solution.py:119
  267.5 0.7 slice_add_fusion.2
  268.3 13.5 %all-gather.9 = f32[4,4,384]{2,1,0:T(4,128)S(1)} all-gather(f32[1,4,384]{2,1,0:T(4,128)S(1)} %maximum_bitcast_fusion.1), channel_id=7, replica_groups=mesh['grp'=2,'sp'=4,'tp'=4] {'sp'}, dimensions={0}, use_global_device_ids=true | all-gather | bytes 30720 | tf_op jit(solution)/shard_map/all_gather | solution.py:129
  281.9 20.9 %all-gather.33.cloned.1.call-done = bf16[1,384,2048]{2,1,0:T(8,128)(2,1)} async-done(((bf16[1,384,512]{2,1,0:T(8,128)(2,1)}), bf16[1,384,2048]{2,1,0:T(8,128)(2,1)}) %all-gather.33.cloned.1.call-update) | async-done | bytes 1572880 | tf_op jit(solution)/shard_map/all_gather | solution.py:134
  302.8 4.7 %convolution_convert_fusion = bf16[256,2048]{1,0:T(8,128)(2,1)} fusion(bf16[1,384,2048]{2,1,0:T(8,128)(2,1)} %all-gather.33.cloned.1.call-done, bf16[1,2048,384]{2,1,0:T(8,128)(2,1)} %all-gather.31.cloned.1.call-done, f32[256,384]{1,0:T(8,128)} %rev.19, f32[256,384]{1,0:T(8,128)} %rev.18, f32[256,384]{1,0:T(8,128)S(1)} %pad.486, f32[256,384]{1,0:T(8,128)S(1)} %pad.487, ...), kind=kOutput, calls=%fused_computation.4 | convolution fusion | flops 809795584 | bytes 7614464 | tf_op jit(solution)/shard_map/dot_general | solution.py:132
  307.4 23.8 %reduce-scatter.5.cloned.1.call-done = bf16[256,512]{1,0:T(8,128)(2,1)} async-done(((bf16[256,2048]{1,0:T(8,128)(2,1)}), bf16[256,512]{1,0:T(8,128)(2,1)}) %reduce-scatter.5.cloned.1.call-update) | async-done | bytes 262160 | tf_op jit(solution)/shard_map/reduce_scatter | solution.py:137
  331.2 1.7 add_convert_fusion
  (630 shorter events, 23.1 us)
Async XLA Ops:
  6.5 3.0 copy-start.8
  6.5 21.8 %all-gather.19.cloned.1.call-start = ((), (), s32[]{:S(2)}) async-start(), calls=%async_computation.2 | async-start | bytes 1310720 | tf_op jit(solution)/shard_map/all_gather | solution.py:71
  7.3 59.7 %all-gather.23.cloned.1.call-start = ((), (), s32[]{:S(2)}) async-start(), calls=%async_computation.6 | async-start | bytes 1966080 | tf_op jit(solution)/shard_map/all_gather | solution.py:75
  9.4 1.3 copy-start.9
  9.4 112.5 %all-gather.25.cloned.1.call-start = ((), (), s32[]{:S(2)}) async-start(), calls=%async_computation.7 | async-start | bytes 1966080 | tf_op jit(solution)/shard_map/all_gather | solution.py:80
  10.5 1.3 copy-start.27
  10.5 1.9 copy-start.28
  10.5 2.5 copy-start.31
  10.5 3.1 copy-start.37
  10.5 131.5 %all-gather.27.cloned.1.call-start = ((), (), s32[]{:S(2)}) async-start(), calls=%async_computation.8 | async-start | bytes 1966080 | tf_op jit(solution)/shard_map/all_gather | solution.py:134
  11.7 158.8 %reduce-scatter.3.cloned.1.call-start = ((), (), s32[]{:S(2)}) async-start(), calls=%async_computation.3 | async-start | bytes 1310720 | tf_op jit(solution)/shard_map/reduce_scatter | solution.py:137
  12.4 57.1 %copy-start.18 = (f32[1,2048]{1,0:T(1,128)}, f32[1,2048]{1,0:T(1,128)S(1)}, u32[]{:S(2)}) copy-start(f32[1,2048]{1,0:T(1,128)S(1)} %get-tuple-element.124) | copy-start | bytes 24580
  13.0 64.7 %copy-start.23 = (f32[384]{0:T(512)}, f32[384]{0:T(512)S(1)}, u32[]{:S(2)}) copy-start(f32[384]{0:T(512)S(1)} %get-tuple-element.27) | copy-start | bytes 4612
  13.0 64.7 %copy-start.24 = (f32[384]{0:T(512)}, f32[384]{0:T(512)S(1)}, u32[]{:S(2)}) copy-start(f32[384]{0:T(512)S(1)} %get-tuple-element.28) | copy-start | bytes 4612
  13.0 64.7 %copy-start.25 = (f32[384]{0:T(512)}, f32[384]{0:T(512)S(1)}, u32[]{:S(2)}) copy-start(f32[384]{0:T(512)S(1)} %get-tuple-element.29) | copy-start | bytes 4612
  13.0 64.7 %copy-start.26 = (f32[384]{0:T(512)}, f32[384]{0:T(512)S(1)}, u32[]{:S(2)}) copy-start(f32[384]{0:T(512)S(1)} %get-tuple-element.30) | copy-start | bytes 4612
  29.9 39.6 %copy-start.35 = (f32[256]{0:T(256)}, f32[256]{0:T(256)S(1)}, u32[]{:S(2)}) copy-start(f32[256]{0:T(256)S(1)} %add_rsqrt_fusion.1) | copy-start | bytes 3076
  69.5 8.6 %copy-start.38 = (bf16[2,2,2,3,128,128]{5,4,3,2,1,0:T(8,128)(2,1)S(1)}, bf16[2,2,2,3,128,128]{5,4,3,2,1,0:T(8,128)(2,1)}, u32[]{:S(2)}) copy-start(bf16[2,2,2,3,128,128]{5,4,3,2,1,0:T(8,128)(2,1)} %param.15) | copy-start | bytes 2359300
  69.5 4.5 %collective-permute-start = (bf16[2,384]{1,0:T(2,128)(2,1)S(1)}, bf16[2,384]{1,0:T(2,128)(2,1)S(1)}, u32[]{:S(2)}, u32[]{:S(2)}) collective-permute-start(bf16[2,384]{1,0:T(2,128)(2,1)S(1)} %get-tuple-element.73), channel_id=1, source_target_pairs={{0,4},{4,8},{8,12},{1,5},{5,9},{9,13},{2,6},{6,10},{10,14},{3,7},{... | collective-permute-start | bytes 4616 | tf_op jit(solution)/shard_map/ppermute | solution.py:18
  72.1 5.5 %collective-permute-start.1 = (bf16[2,384]{1,0:T(2,128)(2,1)S(1)}, bf16[2,384]{1,0:T(2,128)(2,1)S(1)}, u32[]{:S(2)}, u32[]{:S(2)}) collective-permute-start(bf16[2,384]{1,0:T(2,128)(2,1)S(1)} %get-tuple-element.74), channel_id=1, source_target_pairs={{4,0},{8,4},{12,8},{5,1},{9,5},{13,9},{6,2},{10,6},{14,10},{7,3},{... | collective-permute-start | bytes 4616 | tf_op jit(solution)/shard_map/ppermute | solution.py:20
  87.5 0.7 copy-start.32
  89.9 1.6 copy-start.10
  91.2 0.9 copy-start.12
  91.3 0.9 copy-start.14
  95.5 1.8 copy-start.4
  97.3 0.8 copy-start.6
  98.9 43.1 %copy-start = (bf16[256,2048]{1,0:T(8,128)(2,1)S(1)}, bf16[256,2048]{1,0:T(8,128)(2,1)}, u32[]{:S(2)}) copy-start(bf16[256,2048]{1,0:T(8,128)(2,1)} %all-gather.19.cloned.1.call-done) | copy-start | bytes 3145732
  98.9 43.1 %copy-start.19 = (f32[1,2048]{1,0:T(1,128)S(1)}, f32[1,2048]{1,0:T(1,128)}, u32[]{:S(2)}) copy-start(f32[1,2048]{1,0:T(1,128)} %copy-done.18) | copy-start | bytes 24580
  98.9 43.1 %copy-start.36 = (f32[256]{0:T(256)S(1)}, f32[256]{0:T(256)}, u32[]{:S(2)}) copy-start(f32[256]{0:T(256)} %copy-done.35) | copy-start | bytes 3076
  121.9 48.5 %copy-start.7 = (bf16[256,512]{1,0:T(8,128)(2,1)S(1)}, bf16[256,512]{1,0:T(8,128)(2,1)}, u32[]{:S(2)}) copy-start(bf16[256,512]{1,0:T(8,128)(2,1)} %param.9) | copy-start | bytes 786436
  146.7 81.0 %copy-start.16 = (f32[1,2048]{1,0:T(1,128)S(1)}, f32[1,2048]{1,0:T(1,128)}, u32[]{:S(2)}) copy-start(f32[1,2048]{1,0:T(1,128)} %get-tuple-element.123) | copy-start | bytes 24580
  146.7 42.3 %all-gather.21.cloned.1.call-start = ((), (), s32[]{:S(2)}) async-start(), calls=%async_computation.4 | async-start | bytes 1310720 | tf_op jit(solution)/shard_map/all_gather | solution.py:71
  172.2 55.5 %all-gather.29.cloned.1.call-start = ((), (), s32[]{:S(2)}) async-start(), calls=%async_computation.9 | async-start | bytes 1966080 | tf_op jit(solution)/shard_map/all_gather | solution.py:75
  172.9 108.9 %all-gather.31.cloned.1.call-start = ((), (), s32[]{:S(2)}) async-start(), calls=%async_computation.10 | async-start | bytes 1966080 | tf_op jit(solution)/shard_map/all_gather | solution.py:80
  173.7 129.1 %all-gather.33.cloned.1.call-start = ((), (), s32[]{:S(2)}) async-start(), calls=%async_computation.11 | async-start | bytes 1966080 | tf_op jit(solution)/shard_map/all_gather | solution.py:134
  174.4 156.8 %reduce-scatter.5.cloned.1.call-start = ((), (), s32[]{:S(2)}) async-start(), calls=%async_computation.5 | async-start | bytes 1310720 | tf_op jit(solution)/shard_map/reduce_scatter | solution.py:137
  190.5 39.6 %copy-start.33 = (f32[256]{0:T(256)}, f32[256]{0:T(256)S(1)}, u32[]{:S(2)}) copy-start(f32[256]{0:T(256)S(1)} %add_rsqrt_fusion) | copy-start | bytes 3076
  227.7 6.5 %copy-start.29 = (f32[384]{0:T(512)S(1)}, f32[384]{0:T(512)}, u32[]{:S(2)}) copy-start(f32[384]{0:T(512)} %get-tuple-element.33) | copy-start | bytes 4612
  227.7 6.5 %copy-start.30 = (f32[384]{0:T(512)S(1)}, f32[384]{0:T(512)}, u32[]{:S(2)}) copy-start(f32[384]{0:T(512)} %get-tuple-element.36) | copy-start | bytes 4612
  227.7 10.7 %copy-start.20 = (f32[384]{0:T(512)S(1)}, f32[384]{0:T(512)}, u32[]{:S(2)}) copy-start(f32[384]{0:T(512)} %get-tuple-element.26) | copy-start | bytes 4612
  227.7 10.7 %copy-start.21 = (f32[384]{0:T(512)S(1)}, f32[384]{0:T(512)}, u32[]{:S(2)}) copy-start(f32[384]{0:T(512)} %get-tuple-element.31) | copy-start | bytes 4612
  227.7 10.7 %copy-start.22 = (f32[384]{0:T(512)S(1)}, f32[384]{0:T(512)}, u32[]{:S(2)}) copy-start(f32[384]{0:T(512)} %get-tuple-element.32) | copy-start | bytes 4612
  230.2 8.6 %copy-start.39 = (bf16[2,2,2,3,128,128]{5,4,3,2,1,0:T(8,128)(2,1)S(1)}, bf16[2,2,2,3,128,128]{5,4,3,2,1,0:T(8,128)(2,1)}, u32[]{:S(2)}) copy-start(bf16[2,2,2,3,128,128]{5,4,3,2,1,0:T(8,128)(2,1)} %param.15) | copy-start | bytes 2359300
  230.2 4.6 %collective-permute-start.2 = (bf16[2,384]{1,0:T(2,128)(2,1)S(1)}, bf16[2,384]{1,0:T(2,128)(2,1)S(1)}, u32[]{:S(2)}, u32[]{:S(2)}) collective-permute-start(bf16[2,384]{1,0:T(2,128)(2,1)S(1)} %get-tuple-element.61), channel_id=1, source_target_pairs={{0,4},{4,8},{8,12},{1,5},{5,9},{9,13},{2,6},{6,10},{10,14},{3,7},{... | collective-permute-start | bytes 4616 | tf_op jit(solution)/shard_map/ppermute | solution.py:18
  232.8 5.5 %collective-permute-start.3 = (bf16[2,384]{1,0:T(2,128)(2,1)S(1)}, bf16[2,384]{1,0:T(2,128)(2,1)S(1)}, u32[]{:S(2)}, u32[]{:S(2)}) collective-permute-start(bf16[2,384]{1,0:T(2,128)(2,1)S(1)} %get-tuple-element.62), channel_id=1, source_target_pairs={{4,0},{8,4},{12,8},{5,1},{9,5},{13,9},{6,2},{10,6},{14,10},{7,3},{... | collective-permute-start | bytes 4616 | tf_op jit(solution)/shard_map/ppermute | solution.py:20
  250.0 1.6 copy-start.11
  251.3 0.9 copy-start.13
  251.4 0.9 copy-start.15
  255.6 1.8 copy-start.3
  257.4 0.8 copy-start.5
  258.9 43.8 %copy-start.1 = (bf16[256,2048]{1,0:T(8,128)(2,1)S(1)}, bf16[256,2048]{1,0:T(8,128)(2,1)}, u32[]{:S(2)}) copy-start(bf16[256,2048]{1,0:T(8,128)(2,1)} %all-gather.21.cloned.1.call-done) | copy-start | bytes 3145732
  258.9 43.8 %copy-start.17 = (f32[1,2048]{1,0:T(1,128)S(1)}, f32[1,2048]{1,0:T(1,128)}, u32[]{:S(2)}) copy-start(f32[1,2048]{1,0:T(1,128)} %get-tuple-element.123) | copy-start | bytes 24580
  258.9 43.8 %copy-start.34 = (f32[256]{0:T(256)S(1)}, f32[256]{0:T(256)}, u32[]{:S(2)}) copy-start(f32[256]{0:T(256)} %copy-done.33) | copy-start | bytes 3076
  281.9 49.4 %copy-start.2 = (bf16[256,512]{1,0:T(8,128)(2,1)S(1)}, bf16[256,512]{1,0:T(8,128)(2,1)}, u32[]{:S(2)}) copy-start(bf16[256,512]{1,0:T(8,128)(2,1)} %add_convert_fusion.1) | copy-start | bytes 786436
Sparse Core Ops, SparseCore 0:
  8.9 19.4 all-gather.18
  29.9 37.0 all-gather.22
  68.5 35.8 all-gather.24
  105.9 36.0 all-gather.26
  146.8 23.6 reduce-scatter.2
  172.3 16.6 all-gather.20
  190.6 37.0 all-gather.28
  229.2 35.8 all-gather.30
  266.7 35.9 all-gather.32
  307.6 23.6 reduce-scatter.4
where the time goes:
time: 341 us; the launch traced here: 340 us
  waiting for transfers between devices  201 us (59%)
  local copies, waits for them, and re-layouts  42.5 us (12%)
  other arithmetic  27.8 us (8%)
  blocking collectives  27 us (8%)
  between operations  16.9 us (5%)
  matrix products  16.7 us (5%)
  starting transfers between devices  8.38 us (2%)
    all_gather x2, waiting for transfers between devices, local(): lax.all_gather(convolution_in_weight[layer_index], 'sp', axis=0, tiled=True)  74.2 us
    reduce_scatter x2, waiting for transfers between devices, local(): lax.psum_scatter(partials.astype(jnp.float32).astype(jnp.bfloat16), 'tp',...  47.5 us
    all_gather x2, waiting for transfers between devices, local(): lax.all_gather(output_weight[layer_index], 'sp', axis=1, tiled=True)  40.9 us
    all_gather x2, waiting for transfers between devices, local(): features = lax.all_gather(stream, 'tp', axis=1, tiled=True)  28.1 us
    all_gather x2, blocking collectives, local(): lax.all_gather(ends, 'sp')  27 us
    rev x4, local copies, waits for them, and re-layouts, local(): lax.associative_scan(combine_pairs, (jnp.exp(decay_logarithm), driven), r...  15.6 us
    add x68, other arithmetic, local(): lax.associative_scan(combine_pairs, (jnp.exp(decay_logarithm), driven), r...  10.5 us
    dot_general x2, matrix products, local(): jnp.dot(gated, lax.all_gather(output_weight[layer_index], 'sp', axis=1, t...  9.31 us
  transfers between devices with their start and end apart: 14, of which 10 were waited for; matrix products, arithmetic and copies ran while one was open for 21% of the time, Pallas kernels for 0%

commit v1 on v0

--- a/solution.py
+++ b/solution.py
@@ -68,7 +68,13 @@
     at_first = (positions == 0)[:, None]
     at_last = (positions == seq_length - 1)[:, None]
     for layer_index in range(convolution_in_weight.shape[0]):
-        features = lax.all_gather(stream, "tp", axis=1, tiled=True)
+        count_2 = lax.axis_size("tp")
+        held, pieces = (stream, [stream])
+        for _ in range(count_2 - 1):
+            held = lax.ppermute(held, "tp", [(i_2, (i_2 + 1) % count_2) for i_2 in range(count_2)])
+            pieces.insert(0, held)
+        line = jnp.concatenate(pieces, axis=1)
+        features = jnp.roll(line, (lax.axis_index("tp") + 1) * stream.shape[1], axis=1)
         normed = rms_norm(features, layer_norm_gain[layer_index])
         acc_x = jnp.dot(
             normed,

time: 341 us -> 436 us (1.28)
  local copies, waits for them, and re-layouts: 42.5 us -> 149 us
  waiting for transfers between devices: 201 us -> 122 us
  other arithmetic: 27.8 us -> 84.8 us
  matrix products: 16.7 us -> 23.3 us
    slice x220, local copies, waits for them, and re-layouts: 8.85 us -> 91.2 us  [local(): lax.associative_scan(combine_pairs, (jnp.exp(decay_logarithm), driven), r...]
    all_gather x2, waiting for transfers between devices: 40.9 us -> 0.04 us  [local(): lax.all_gather(output_weight[layer_index], 'sp', axis=1, tiled=True)]
    all_gather x2, waiting for transfers between devices: 74.2 us -> 35 us  [local(): lax.all_gather(convolution_in_weight[layer_index], 'sp', axis=0, tiled=True)]
    ppermute x0 -> x6, waiting for transfers between devices: none -> 31.1 us  [local(): lax.ppermute(held, 'tp', [(i_2, (i_2 + 1) % count_2) for i_2 in range(cou...]
    all_gather x2 -> x0, waiting for transfers between devices: 28.1 us -> none  [local(): features = lax.all_gather(stream, 'tp', axis=1, tiled=True)]
    pad x112, local copies, waits for them, and re-layouts: 7.85 us -> 29.4 us  [local(): lax.associative_scan(combine_pairs, (jnp.exp(decay_logarithm), driven), r...]
    add x52, other arithmetic: 2.3 us -> 22.6 us  [combine_pairs(): return (earlier[0] * latter[0], latter[0] * earlier[1] + latter[1])]
    concatenate x56, other arithmetic: 2.07 us -> 19.9 us  [local(): lax.associative_scan(combine_pairs, (jnp.exp(decay_logarithm), driven), r...]
  transfers between devices with their start and end apart: 14 -> 18, of which waited for: 10 -> 12; matrix products, arithmetic and copies ran while one was open for 21% -> 57% of each run, Pallas kernels for 0% -> 0%
where the time goes in v1:
time: 436 us; the launch traced here: 431 us
  local copies, waits for them, and re-layouts  149 us (34%)
  waiting for transfers between devices  122 us (28%)
  other arithmetic  84.8 us (19%)
  blocking collectives  26.3 us (6%)
  matrix products  23.3 us (5%)
  between operations  16.6 us (4%)
  starting transfers between devices  8.86 us (2%)
    slice x220, local copies, waits for them, and re-layouts, local(): lax.associative_scan(combine_pairs, (jnp.exp(decay_logarithm), driven), r...  91.2 us
    reduce_scatter x2, waiting for transfers between devices, local(): lax.psum_scatter(partials.astype(jnp.float32).astype(jnp.bfloat16), 'tp',...  46.5 us
    all_gather x2, waiting for transfers between devices, local(): lax.all_gather(convolution_in_weight[layer_index], 'sp', axis=0, tiled=True)  35 us
    ppermute x6, waiting for transfers between devices, local(): lax.ppermute(held, 'tp', [(i_2, (i_2 + 1) % count_2) for i_2 in range(cou...  31.1 us
    pad x112, local copies, waits for them, and re-layouts, local(): lax.associative_scan(combine_pairs, (jnp.exp(decay_logarithm), driven), r...  29.4 us
    all_gather x2, blocking collectives, local(): lax.all_gather(ends, 'sp')  26.3 us
    add x68, other arithmetic, local(): lax.associative_scan(combine_pairs, (jnp.exp(decay_logarithm), driven), r...  24.8 us
    add x52, other arithmetic, combine_pairs(): return (earlier[0] * latter[0], latter[0] * earlier[1] + latter[1])  22.6 us
  transfers between devices with their start and end apart: 18, of which 12 were waited for; matrix products, arithmetic and copies ran while one was open for 57% of the time, Pallas kernels for 0%

profile of v1, /device:TPU:0, one launch (start us, length us, event | category | flops | bytes accessed | tf_op | source)
XLA Modules:
  0.0 431.2 jit_solution(11274290968168247839)
XLA Ops:
  6.5 2.2 fusion.226
  12.0 4.3 %collective-permute-done = bf16[256,512]{1,0:T(8,128)(2,1)S(1)} collective-permute-done((bf16[256,512]{1,0:T(8,128)(2,1)S(1)}, bf16[256,512]{1,0:T(8,128)(2,1)S(1)}, u32[]{:S(2)}, u32[]{:S(2)}) %collective-permute-start) | collective-permute-done | bytes 262176 | tf_op jit(solution)/shard_map/ppermute | solution.py:74
  17.6 4.6 %collective-permute-done.1 = bf16[256,512]{1,0:T(8,128)(2,1)S(1)} collective-permute-done((bf16[256,512]{1,0:T(8,128)(2,1)S(1)}, bf16[256,512]{1,0:T(8,128)(2,1)S(1)}, u32[]{:S(2)}, u32[]{:S(2)}) %collective-permute-start.1) | collective-permute-done | bytes 262176 | tf_op jit(solution)/shard_map/ppermute | solution.py:74
  22.8 5.2 %collective-permute-done.2 = bf16[256,512]{1,0:T(8,128)(2,1)S(1)} collective-permute-done((bf16[256,512]{1,0:T(8,128)(2,1)S(1)}, bf16[256,512]{1,0:T(8,128)(2,1)S(1)}, u32[]{:S(2)}, u32[]{:S(2)}) %collective-permute-start.2) | collective-permute-done | bytes 262176 | tf_op jit(solution)/shard_map/ppermute | solution.py:74
  28.0 2.8 fusion
  30.8 17.8 %all-gather.17.cloned.1.call-done = bf16[1,2048,384]{2,1,0:T(8,128)(2,1)} async-done(((bf16[1,512,384]{2,1,0:T(8,128)(2,1)}), bf16[1,2048,384]{2,1,0:T(8,128)(2,1)}) %all-gather.17.cloned.1.call-update) | async-done | bytes 1572880 | tf_op jit(solution)/shard_map/all_gather | solution.py:81
  48.7 2.2 fusion.40
  50.9 2.5 collective-permute-start.3
  53.4 1.5 collective-permute-start.4
  54.9 3.9 collective-permute-done.4
  67.1 2.1 convert_multiply_fusion.7
  125.4 1.6 pad.439
  127.1 2.4 slice.1364
  129.5 2.4 slice.1406
  132.6 1.8 fusion.140
  134.5 2.5 pad.455
  137.0 1.7 pad_maximum_fusion.3
  138.6 2.6 pad.454
  141.3 1.9 add.1036
  143.2 3.9 rev.16
  147.9 3.9 rev.17
  152.5 13.2 %all-gather.8 = f32[4,4,384]{2,1,0:T(4,128)S(1)} all-gather(f32[1,4,384]{2,1,0:T(4,128)S(1)} %maximum_bitcast_fusion), channel_id=3, replica_groups=mesh['grp'=2,'sp'=4,'tp'=4] {'sp'}, dimensions={0}, use_global_device_ids=true | all-gather | bytes 30720 | tf_op jit(solution)/shard_map/all_gather | solution.py:135
  165.8 4.7 %convolution_convert_fusion.1 = bf16[256,2048]{1,0:T(8,128)(2,1)} fusion(bf16[1,384,2048]{2,1,0:T(8,128)(2,1)} %all-gather.21.cloned.1.call-done, bf16[1,2048,384]{2,1,0:T(8,128)(2,1)} %all-gather.19.cloned.1.call-done, f32[256,384]{1,0:T(8,128)} %rev.17, f32[256,384]{1,0:T(8,128)} %rev.16, f32[256,384]{1,0:T(8,128)S(1)} %pad.422, f32[256,384]{1,0:T(8,128)S(1)} %pad.423, ...), kind=kOutput, calls=%fused_computation.5 | convolution fusion | flops 809795584 | bytes 7614464 | tf_op jit(solution)/shard_map/dot_general | solution.py:138
  171.8 22.6 %reduce-scatter.3.cloned.1.call-done = bf16[256,512]{1,0:T(8,128)(2,1)} async-done(((bf16[256,2048]{1,0:T(8,128)(2,1)}), bf16[256,512]{1,0:T(8,128)(2,1)}) %reduce-scatter.3.cloned.1.call-update) | async-done | bytes 262160 | tf_op jit(solution)/shard_map/reduce_scatter | solution.py:143
  195.5 5.8 %collective-permute-done.5 = bf16[256,512]{1,0:T(8,128)(2,1)S(1)} collective-permute-done((bf16[256,512]{1,0:T(8,128)(2,1)S(1)}, bf16[256,512]{1,0:T(8,128)(2,1)S(1)}, u32[]{:S(2)}, u32[]{:S(2)}) %collective-permute-start.5) | collective-permute-done | bytes 262176 | tf_op jit(solution)/shard_map/ppermute | solution.py:74
  201.3 5.8 %collective-permute-done.6 = bf16[256,512]{1,0:T(8,128)(2,1)S(1)} collective-permute-done((bf16[256,512]{1,0:T(8,128)(2,1)S(1)}, bf16[256,512]{1,0:T(8,128)(2,1)S(1)}, u32[]{:S(2)}, u32[]{:S(2)}) %collective-permute-start.6) | collective-permute-done | bytes 262176 | tf_op jit(solution)/shard_map/ppermute | solution.py:74
  207.4 5.5 %collective-permute-done.7 = bf16[256,512]{1,0:T(8,128)(2,1)S(1)} collective-permute-done((bf16[256,512]{1,0:T(8,128)(2,1)S(1)}, bf16[256,512]{1,0:T(8,128)(2,1)S(1)}, u32[]{:S(2)}, u32[]{:S(2)}) %collective-permute-start.7) | collective-permute-done | bytes 262176 | tf_op jit(solution)/shard_map/ppermute | solution.py:74
  212.9 2.8 fusion.3
  215.8 17.2 %all-gather.23.cloned.1.call-done = bf16[1,2048,384]{2,1,0:T(8,128)(2,1)} async-done(((bf16[1,512,384]{2,1,0:T(8,128)(2,1)}), bf16[1,2048,384]{2,1,0:T(8,128)(2,1)}) %all-gather.23.cloned.1.call-update) | async-done | bytes 1572880 | tf_op jit(solution)/shard_map/all_gather | solution.py:81
  233.0 2.2 fusion.49
  235.2 2.5 collective-permute-start.8
  239.0 4.1 collective-permute-done.9
  252.2 2.3 convert_multiply_fusion.5
  264.2 1.5 multiply_add_fusion.13
  267.0 1.4 slice.1458
  268.4 1.4 slice.1462
  269.8 1.4 multiply_add_fusion.17
  272.4 1.3 slice.1464
  273.7 1.3 slice.1468
  275.0 1.4 multiply_add_fusion.21
  276.4 1.3 slice.1471
  277.7 1.3 slice.1472
  279.0 1.3 slice.1470
  280.3 1.3 slice.1474
  281.6 1.3 multiply_add_fusion.25
  285.5 1.3 slice.1480
  288.1 1.4 fusion.232
  290.8 1.3 slice.1486
  294.6 1.3 slice.1463
  337.1 1.4 fusion.174
  339.3 2.1 pad.499
  351.4 1.6 pad.470
  353.1 1.6 pad.503
  356.5 2.4 slice.1556
  362.1 1.6 pad.502
  365.4 2.5 pad.518
  367.9 1.8 add.1130
  369.7 3.9 rev.18
  373.6 1.8 add.1105
  375.5 3.9 rev.19
  380.8 13.2 %all-gather.9 = f32[4,4,384]{2,1,0:T(4,128)S(1)} all-gather(f32[1,4,384]{2,1,0:T(4,128)S(1)} %maximum_bitcast_fusion.1), channel_id=7, replica_groups=mesh['grp'=2,'sp'=4,'tp'=4] {'sp'}, dimensions={0}, use_global_device_ids=true | all-gather | bytes 30720 | tf_op jit(solution)/shard_map/all_gather | solution.py:135
  394.1 4.6 %convolution_convert_fusion = bf16[256,2048]{1,0:T(8,128)(2,1)} fusion(bf16[1,384,2048]{2,1,0:T(8,128)(2,1)} %all-gather.27.cloned.1.call-done, bf16[1,2048,384]{2,1,0:T(8,128)(2,1)} %all-gather.25.cloned.1.call-done, f32[256,384]{1,0:T(8,128)} %rev.19, f32[256,384]{1,0:T(8,128)} %rev.18, f32[256,384]{1,0:T(8,128)S(1)} %pad.486, f32[256,384]{1,0:T(8,128)S(1)} %pad.487, ...), kind=kOutput, calls=%fused_computation.4 | convolution fusion | flops 809795584 | bytes 7614464 | tf_op jit(solution)/shard_map/dot_general | solution.py:138
  398.8 23.8 %reduce-scatter.5.cloned.1.call-done = bf16[256,512]{1,0:T(8,128)(2,1)} async-done(((bf16[256,2048]{1,0:T(8,128)(2,1)}), bf16[256,512]{1,0:T(8,128)(2,1)}) %reduce-scatter.5.cloned.1.call-update) | async-done | bytes 262160 | tf_op jit(solution)/shard_map/reduce_scatter | solution.py:143
  422.6 1.7 add_convert_fusion
  (762 shorter events, 162.7 us)
Async XLA Ops:
  6.5 42.1 %all-gather.17.cloned.1.call-start = ((), (), s32[]{:S(2)}) async-start(), calls=%async_computation.4 | async-start | bytes 1966080 | tf_op jit(solution)/shard_map/all_gather | solution.py:81
  8.7 157.1 %all-gather.19.cloned.1.call-start = ((), (), s32[]{:S(2)}) async-start(), calls=%async_computation.5 | async-start | bytes 1966080 | tf_op jit(solution)/shard_map/all_gather | solution.py:86
  9.8 12.4 %copy-start.71 = (f32[2,2,384]{2,1,0:T(2,128)S(1)}, f32[2,2,384]{2,1,0:T(2,128)}, u32[]{:S(2)}) copy-start(f32[2,2,384]{2,1,0:T(2,128)} %param.18) | copy-start | bytes 18436
  9.8 156.0 %all-gather.21.cloned.1.call-start = ((), (), s32[]{:S(2)}) async-start(), calls=%async_computation.6 | async-start | bytes 1966080 | tf_op jit(solution)/shard_map/all_gather | solution.py:140
  9.9 6.5 %collective-permute-start = (bf16[256,512]{1,0:T(8,128)(2,1)S(1)}, bf16[256,512]{1,0:T(8,128)(2,1)S(1)}, u32[]{:S(2)}, u32[]{:S(2)}) collective-permute-start(bf16[256,512]{1,0:T(8,128)(2,1)S(1)} %copy-done.4), channel_id=1, source_target_pairs={{0,1},{1,2},{2,3},{3,0},{4,5},{5,6},{6,7},{7,4},{8,9},{9,10},{10,1... | collective-permute-start | bytes 786440 | tf_op jit(solution)/shard_map/ppermute | solution.py:74
  11.4 183.1 %reduce-scatter.3.cloned.1.call-start = ((), (), s32[]{:S(2)}) async-start(), calls=%async_computation.2 | async-start | bytes 1310720 | tf_op jit(solution)/shard_map/reduce_scatter | solution.py:143
  12.0 38.8 %copy-start.41 = (f32[1,2048]{1,0:T(1,128)}, f32[1,2048]{1,0:T(1,128)S(1)}, u32[]{:S(2)}) copy-start(f32[1,2048]{1,0:T(1,128)S(1)} %get-tuple-element.129) | copy-start | bytes 24580
  16.4 5.8 %collective-permute-start.1 = (bf16[256,512]{1,0:T(8,128)(2,1)S(1)}, bf16[256,512]{1,0:T(8,128)(2,1)S(1)}, u32[]{:S(2)}, u32[]{:S(2)}) collective-permute-start(bf16[256,512]{1,0:T(8,128)(2,1)S(1)} %collective-permute-done), channel_id=1, source_target_pairs={{0,1},{1,2},{2,3},{3,0},{4,5},{5,6},{6,7},{7,4},{8,9},{9,10},{10,1... | collective-permute-start | bytes 786440 | tf_op jit(solution)/shard_map/ppermute | solution.py:74
  22.2 5.8 %collective-permute-start.2 = (bf16[256,512]{1,0:T(8,128)(2,1)S(1)}, bf16[256,512]{1,0:T(8,128)(2,1)S(1)}, u32[]{:S(2)}, u32[]{:S(2)}) collective-permute-start(bf16[256,512]{1,0:T(8,128)(2,1)S(1)} %collective-permute-done.1), channel_id=1, source_target_pairs={{0,1},{1,2},{2,3},{3,0},{4,5},{5,6},{6,7},{7,4},{8,9},{9,10},{10,1... | collective-permute-start | bytes 786440 | tf_op jit(solution)/shard_map/ppermute | solution.py:74
  30.8 20.0 %copy-start.94 = (f32[256]{0:T(256)}, f32[256]{0:T(256)S(1)}, u32[]{:S(2)}) copy-start(f32[256]{0:T(256)S(1)} %add_rsqrt_fusion.1) | copy-start | bytes 3076
  50.9 4.0 collective-permute-start.3
  53.4 5.5 %collective-permute-start.4 = (bf16[2,384]{1,0:T(2,128)(2,1)S(1)}, bf16[2,384]{1,0:T(2,128)(2,1)S(1)}, u32[]{:S(2)}, u32[]{:S(2)}) collective-permute-start(bf16[2,384]{1,0:T(2,128)(2,1)S(1)} %get-tuple-element.79), channel_id=1, source_target_pairs={{4,0},{8,4},{12,8},{5,1},{9,5},{13,9},{6,2},{10,6},{14,10},{7,3},{... | collective-permute-start | bytes 4616 | tf_op jit(solution)/shard_map/ppermute | solution.py:20
  89.6 12.2 %copy-start.53 = (f32[2,384]{1,0:T(2,128)S(1)}, f32[2,384]{1,0:T(2,128)}, u32[]{:S(2)}) copy-start(f32[2,384]{1,0:T(2,128)} %pad_add_fusion.6) | copy-start | bytes 9220
  89.6 12.2 %copy-start.55 = (f32[2,384]{1,0:T(2,128)S(1)}, f32[2,384]{1,0:T(2,128)}, u32[]{:S(2)}) copy-start(f32[2,384]{1,0:T(2,128)} %pad_add_fusion.7) | copy-start | bytes 9220
  89.6 12.3 %copy-start.80 = (f32[1,384]{1,0:T(1,128)S(1)}, f32[1,384]{1,0:T(1,128)}, u32[]{:S(2)}) copy-start(f32[1,384]{1,0:T(1,128)} %get-tuple-element.164) | copy-start | bytes 4612
  89.6 12.3 %copy-start.81 = (f32[1,384]{1,0:T(1,128)S(1)}, f32[1,384]{1,0:T(1,128)}, u32[]{:S(2)}) copy-start(f32[1,384]{1,0:T(1,128)} %get-tuple-element.165) | copy-start | bytes 4612
  89.7 12.3 %copy-start.43 = (f32[3,384]{1,0:T(4,128)S(1)}, f32[3,384]{1,0:T(4,128)}, u32[]{:S(2)}) copy-start(f32[3,384]{1,0:T(4,128)} %slice.1277) | copy-start | bytes 13828
  89.7 12.3 %copy-start.44 = (f32[3,384]{1,0:T(4,128)S(1)}, f32[3,384]{1,0:T(4,128)}, u32[]{:S(2)}) copy-start(f32[3,384]{1,0:T(4,128)} %slice.1294) | copy-start | bytes 13828
  89.7 12.3 %copy-start.78 = (f32[1,384]{1,0:T(1,128)S(1)}, f32[1,384]{1,0:T(1,128)}, u32[]{:S(2)}) copy-start(f32[1,384]{1,0:T(1,128)} %slice.1651) | copy-start | bytes 4612
  89.7 12.3 %copy-start.76 = (f32[1,384]{1,0:T(1,128)S(1)}, f32[1,384]{1,0:T(1,128)}, u32[]{:S(2)}) copy-start(f32[1,384]{1,0:T(1,128)} %slice.1625) | copy-start | bytes 4612
  89.7 12.4 %copy-start.35 = (f32[7,384]{1,0:T(8,128)S(1)}, f32[7,384]{1,0:T(8,128)}, u32[]{:S(2)}) copy-start(f32[7,384]{1,0:T(8,128)} %slice.1271) | copy-start | bytes 32260
  89.8 12.4 %copy-start.36 = (f32[7,384]{1,0:T(8,128)S(1)}, f32[7,384]{1,0:T(8,128)}, u32[]{:S(2)}) copy-start(f32[7,384]{1,0:T(8,128)} %slice.1296) | copy-start | bytes 32260
  89.8 12.4 %copy-start.74 = (f32[1,384]{1,0:T(1,128)S(1)}, f32[1,384]{1,0:T(1,128)}, u32[]{:S(2)}) copy-start(f32[1,384]{1,0:T(1,128)} %slice.1650) | copy-start | bytes 4612
  89.8 12.4 %copy-start.72 = (f32[1,384]{1,0:T(1,128)S(1)}, f32[1,384]{1,0:T(1,128)}, u32[]{:S(2)}) copy-start(f32[1,384]{1,0:T(1,128)} %slice.1624) | copy-start | bytes 4612
  89.8 12.5 %copy-start.28 = (f32[15,384]{1,0:T(8,128)S(1)}, f32[15,384]{1,0:T(8,128)}, u32[]{:S(2)}) copy-start(f32[15,384]{1,0:T(8,128)} %slice.1265) | copy-start | bytes 69124
  89.8 12.5 %copy-start.29 = (f32[15,384]{1,0:T(8,128)S(1)}, f32[15,384]{1,0:T(8,128)}, u32[]{:S(2)}) copy-start(f32[15,384]{1,0:T(8,128)} %slice.1298) | copy-start | bytes 69124
  89.8 12.5 %copy-start.69 = (f32[1,384]{1,0:T(1,128)S(1)}, f32[1,384]{1,0:T(1,128)}, u32[]{:S(2)}) copy-start(f32[1,384]{1,0:T(1,128)} %slice.1649) | copy-start | bytes 4612
  89.9 12.5 %copy-start.67 = (f32[1,384]{1,0:T(1,128)S(1)}, f32[1,384]{1,0:T(1,128)}, u32[]{:S(2)}) copy-start(f32[1,384]{1,0:T(1,128)} %slice.1623) | copy-start | bytes 4612
  90.1 12.4 %copy-start.90 = (f32[1,384]{1,0:T(1,128)S(1)}, f32[1,384]{1,0:T(1,128)}, u32[]{:S(2)}) copy-start(f32[1,384]{1,0:T(1,128)} %slice.1648) | copy-start | bytes 4612
  143.2 22.7 %copy-start.42 = (f32[1,2048]{1,0:T(1,128)S(1)}, f32[1,2048]{1,0:T(1,128)}, u32[]{:S(2)}) copy-start(f32[1,2048]{1,0:T(1,128)} %copy-done.41) | copy-start | bytes 24580
  143.2 22.7 %copy-start.95 = (f32[256]{0:T(256)S(1)}, f32[256]{0:T(256)}, u32[]{:S(2)}) copy-start(f32[256]{0:T(256)} %copy-done.94) | copy-start | bytes 3076
  170.6 23.9 %copy-start.5 = (bf16[256,512]{1,0:T(8,128)(2,1)S(1)}, bf16[256,512]{1,0:T(8,128)(2,1)}, u32[]{:S(2)}) copy-start(bf16[256,512]{1,0:T(8,128)(2,1)} %param.11) | copy-start | bytes 786436
  170.6 62.3 %all-gather.23.cloned.1.call-start = ((), (), s32[]{:S(2)}) async-start(), calls=%async_computation.7 | async-start | bytes 1966080 | tf_op jit(solution)/shard_map/all_gather | solution.py:81
  171.2 222.9 %all-gather.25.cloned.1.call-start = ((), (), s32[]{:S(2)}) async-start(), calls=%async_computation.8 | async-start | bytes 1966080 | tf_op jit(solution)/shard_map/all_gather | solution.py:86
  171.8 61.2 %copy-start.39 = (f32[1,2048]{1,0:T(1,128)S(1)}, f32[1,2048]{1,0:T(1,128)}, u32[]{:S(2)}) copy-start(f32[1,2048]{1,0:T(1,128)} %get-tuple-element.128) | copy-start | bytes 24580
  171.8 222.3 %all-gather.27.cloned.1.call-start = ((), (), s32[]{:S(2)}) async-start(), calls=%async_computation.9 | async-start | bytes 1966080 | tf_op jit(solution)/shard_map/all_gather | solution.py:140
  195.5 5.8 %collective-permute-start.5 = (bf16[256,512]{1,0:T(8,128)(2,1)S(1)}, bf16[256,512]{1,0:T(8,128)(2,1)S(1)}, u32[]{:S(2)}, u32[]{:S(2)}) collective-permute-start(bf16[256,512]{1,0:T(8,128)(2,1)S(1)} %add_convert_fusion.1), channel_id=1, source_target_pairs={{0,1},{1,2},{2,3},{3,0},{4,5},{5,6},{6,7},{7,4},{8,9},{9,10},{10,1... | collective-permute-start | bytes 786440 | tf_op jit(solution)/shard_map/ppermute | solution.py:74
  201.3 5.8 %collective-permute-start.6 = (bf16[256,512]{1,0:T(8,128)(2,1)S(1)}, bf16[256,512]{1,0:T(8,128)(2,1)S(1)}, u32[]{:S(2)}, u32[]{:S(2)}) collective-permute-start(bf16[256,512]{1,0:T(8,128)(2,1)S(1)} %collective-permute-done.5), channel_id=1, source_target_pairs={{0,1},{1,2},{2,3},{3,0},{4,5},{5,6},{6,7},{7,4},{8,9},{9,10},{10,1... | collective-permute-start | bytes 786440 | tf_op jit(solution)/shard_map/ppermute | solution.py:74
  207.1 5.8 %collective-permute-start.7 = (bf16[256,512]{1,0:T(8,128)(2,1)S(1)}, bf16[256,512]{1,0:T(8,128)(2,1)S(1)}, u32[]{:S(2)}, u32[]{:S(2)}) collective-permute-start(bf16[256,512]{1,0:T(8,128)(2,1)S(1)} %collective-permute-done.6), channel_id=1, source_target_pairs={{0,1},{1,2},{2,3},{3,0},{4,5},{5,6},{6,7},{7,4},{8,9},{9,10},{10,1... | collective-permute-start | bytes 786440 | tf_op jit(solution)/shard_map/ppermute | solution.py:74
  207.2 215.5 %reduce-scatter.5.cloned.1.call-start = ((), (), s32[]{:S(2)}) async-start(), calls=%async_computation.3 | async-start | bytes 1310720 | tf_op jit(solution)/shard_map/reduce_scatter | solution.py:143
  215.8 19.4 %copy-start.92 = (f32[256]{0:T(256)}, f32[256]{0:T(256)S(1)}, u32[]{:S(2)}) copy-start(f32[256]{0:T(256)S(1)} %add_rsqrt_fusion) | copy-start | bytes 3076
  235.2 3.8 collective-permute-start.8
  237.7 5.5 %collective-permute-start.9 = (bf16[2,384]{1,0:T(2,128)(2,1)S(1)}, bf16[2,384]{1,0:T(2,128)(2,1)S(1)}, u32[]{:S(2)}, u32[]{:S(2)}) collective-permute-start(bf16[2,384]{1,0:T(2,128)(2,1)S(1)} %get-tuple-element.67), channel_id=1, source_target_pairs={{4,0},{8,4},{12,8},{5,1},{9,5},{13,9},{6,2},{10,6},{14,10},{7,3},{... | collective-permute-start | bytes 4616 | tf_op jit(solution)/shard_map/ppermute | solution.py:20
  308.6 13.4 %copy-start.86 = (f32[1,384]{1,0:T(1,128)S(1)}, f32[1,384]{1,0:T(1,128)}, u32[]{:S(2)}) copy-start(f32[1,384]{1,0:T(1,128)} %get-tuple-element.150) | copy-start | bytes 4612
  308.6 13.4 %copy-start.87 = (f32[1,384]{1,0:T(1,128)S(1)}, f32[1,384]{1,0:T(1,128)}, u32[]{:S(2)}) copy-start(f32[1,384]{1,0:T(1,128)} %get-tuple-element.151) | copy-start | bytes 4612
  308.6 13.4 %copy-start.54 = (f32[2,384]{1,0:T(2,128)S(1)}, f32[2,384]{1,0:T(2,128)}, u32[]{:S(2)}) copy-start(f32[2,384]{1,0:T(2,128)} %pad_add_fusion.2) | copy-start | bytes 9220
  308.6 13.5 %copy-start.56 = (f32[2,384]{1,0:T(2,128)S(1)}, f32[2,384]{1,0:T(2,128)}, u32[]{:S(2)}) copy-start(f32[2,384]{1,0:T(2,128)} %pad_add_fusion.3) | copy-start | bytes 9220
  308.6 13.5 %copy-start.82 = (f32[1,384]{1,0:T(1,128)S(1)}, f32[1,384]{1,0:T(1,128)}, u32[]{:S(2)}) copy-start(f32[1,384]{1,0:T(1,128)} %get-tuple-element.148) | copy-start | bytes 4612
  308.7 13.5 %copy-start.83 = (f32[1,384]{1,0:T(1,128)S(1)}, f32[1,384]{1,0:T(1,128)}, u32[]{:S(2)}) copy-start(f32[1,384]{1,0:T(1,128)} %get-tuple-element.149) | copy-start | bytes 4612
  308.7 13.5 %copy-start.45 = (f32[3,384]{1,0:T(4,128)S(1)}, f32[3,384]{1,0:T(4,128)}, u32[]{:S(2)}) copy-start(f32[3,384]{1,0:T(4,128)} %slice.1486) | copy-start | bytes 13828
  308.7 13.5 %copy-start.79 = (f32[1,384]{1,0:T(1,128)S(1)}, f32[1,384]{1,0:T(1,128)}, u32[]{:S(2)}) copy-start(f32[1,384]{1,0:T(1,128)} %slice.1773) | copy-start | bytes 4612
  308.7 13.6 %copy-start.77 = (f32[1,384]{1,0:T(1,128)S(1)}, f32[1,384]{1,0:T(1,128)}, u32[]{:S(2)}) copy-start(f32[1,384]{1,0:T(1,128)} %slice.1747) | copy-start | bytes 4612
  308.8 13.6 %copy-start.37 = (f32[7,384]{1,0:T(8,128)S(1)}, f32[7,384]{1,0:T(8,128)}, u32[]{:S(2)}) copy-start(f32[7,384]{1,0:T(8,128)} %slice.1463) | copy-start | bytes 32260
  308.8 13.6 %copy-start.38 = (f32[7,384]{1,0:T(8,128)S(1)}, f32[7,384]{1,0:T(8,128)}, u32[]{:S(2)}) copy-start(f32[7,384]{1,0:T(8,128)} %slice.1488) | copy-start | bytes 32260
  308.8 13.6 %copy-start.75 = (f32[1,384]{1,0:T(1,128)S(1)}, f32[1,384]{1,0:T(1,128)}, u32[]{:S(2)}) copy-start(f32[1,384]{1,0:T(1,128)} %slice.1772) | copy-start | bytes 4612
  308.8 13.7 %copy-start.73 = (f32[1,384]{1,0:T(1,128)S(1)}, f32[1,384]{1,0:T(1,128)}, u32[]{:S(2)}) copy-start(f32[1,384]{1,0:T(1,128)} %slice.1746) | copy-start | bytes 4612
  308.9 13.7 %copy-start.30 = (f32[15,384]{1,0:T(8,128)S(1)}, f32[15,384]{1,0:T(8,128)}, u32[]{:S(2)}) copy-start(f32[15,384]{1,0:T(8,128)} %slice.1490) | copy-start | bytes 69124
  308.9 13.7 %copy-start.70 = (f32[1,384]{1,0:T(1,128)S(1)}, f32[1,384]{1,0:T(1,128)}, u32[]{:S(2)}) copy-start(f32[1,384]{1,0:T(1,128)} %slice.1771) | copy-start | bytes 4612
  308.9 13.7 %copy-start.68 = (f32[1,384]{1,0:T(1,128)S(1)}, f32[1,384]{1,0:T(1,128)}, u32[]{:S(2)}) copy-start(f32[1,384]{1,0:T(1,128)} %slice.1745) | copy-start | bytes 4612
  309.0 13.7 %copy-start.26 = (f32[31,384]{1,0:T(8,128)S(1)}, f32[31,384]{1,0:T(8,128)}, u32[]{:S(2)}) copy-start(f32[31,384]{1,0:T(8,128)} %slice.1492) | copy-start | bytes 142852
  309.2 13.6 %copy-start.91 = (f32[1,384]{1,0:T(1,128)S(1)}, f32[1,384]{1,0:T(1,128)}, u32[]{:S(2)}) copy-start(f32[1,384]{1,0:T(1,128)} %slice.1770) | copy-start | bytes 4612
  323.7 13.4 %copy-start.27 = (f32[31,384]{1,0:T(8,128)S(1)}, f32[31,384]{1,0:T(8,128)}, u32[]{:S(2)}) copy-start(f32[31,384]{1,0:T(8,128)} %slice.1551) | copy-start | bytes 142852
  369.7 24.4 %copy-start.40 = (f32[1,2048]{1,0:T(1,128)S(1)}, f32[1,2048]{1,0:T(1,128)}, u32[]{:S(2)}) copy-start(f32[1,2048]{1,0:T(1,128)} %get-tuple-element.128) | copy-start | bytes 24580
  369.7 24.4 %copy-start.93 = (f32[256]{0:T(256)S(1)}, f32[256]{0:T(256)}, u32[]{:S(2)}) copy-start(f32[256]{0:T(256)} %copy-done.92) | copy-start | bytes 3076
  (57 other events, 281.6 us)
Sparse Core Ops, SparseCore 0:
  8.9 39.7 all-gather.16
  50.2 35.8 all-gather.18
  87.7 35.8 all-gather.20
  170.7 23.6 reduce-scatter.2
  195.9 37.0 all-gather.22
  234.4 35.8 all-gather.24
  271.9 35.8 all-gather.26
  398.9 23.6 reduce-scatter.4
